TPU v7x, 32 devices: a whole 2x2x4 slice. The times are simulated.
32 devices in a mesh: sp: 16 (over z, y, core), tp: 2 (over x).
Axes of the slice: x: 2, y: 2, z: 4, core: 2. Of those that a mesh axis runs over, the one named last changes fastest.
Arguments:
- layer_source_rows: bfloat16 [6144, 2048], P(('sp', 'tp')), may hold values from -6 to 6
- entry_rescale_factor: bfloat16 [2048], replicated, may hold values from 0.099609375 to 1.8984375
- sliding_mixer_entry_matrix: bfloat16 [3, 2048, 1024], P(None, 'sp', 'tp'), may hold values from -0.125 to 0.125
- recurrent_mixer_entry_matrix: bfloat16 [2, 2048, 1024], P(None, 'sp', 'tp'), may hold values from -0.125 to 0.125
- latent_write_read_matrix: bfloat16 [2, 2048, 2048], P(None, 'sp', 'tp'), may hold values from -0.125 to 0.125
- timestep_matrix: bfloat16 [2048, 2, 16], P(None, None, 'tp'), may hold values from -0.125 to 0.125
- sliding_kernel_coefficients: bfloat16 [3, 1024], P(None, 'tp'), may hold values from -3.5 to 3.5
- recurrent_kernel_coefficients: bfloat16 [5, 1024], P(None, 'tp'), may hold values from -0.5 to 0.5
- latent_kernel_coefficients: bfloat16 [5, 2, 2048], P(None, None, 'tp'), may hold values from -0.5 to 0.5
- lane_forgetting_rate: float32 [2, 16], P(None, 'tp'), may hold values from 0 to 1
- spike_forgetting_rate: float32 [6144, 16], P('sp', 'tp'), may hold values from -2 to 0
- lane_rescale_factor: bfloat16 [1024], P('tp'), may hold values from 0.099609375 to 1.8984375
- sliding_mixer_exit_matrix: bfloat16 [1024, 2048], P('tp', 'sp'), may hold values from -0.125 to 0.125
- recurrent_mixer_exit_matrix: bfloat16 [1024, 2048], P('tp', 'sp'), may hold values from -0.125 to 0.125
Outputs:
- mixed_out: bfloat16 [6144, 2048], P(('sp', 'tp'))
All inputs are finite; a program needn't handle non-finite values.
Results may differ from a plain program's by a relative error of at most 0.017.
Values may be sent and summed in bfloat16 or wider, within the bound.
No kernel may reach another device: no remote copies, remote signals or barrier semaphores. Data moves between devices by JAX's collectives and lax.ppermute only.
A program may use at most 64 MiB of HBM per device.

v0:
```python
import jax
import jax.numpy as jnp
from jax import lax
from jax.sharding import PartitionSpec as P

HEAD_DIM = 64
STATE = 128
BLOCK = 128


epsilon = 1e-05


def carried_in(value, axis, join, neutral):
    count, mine = (lax.axis_size(axis), lax.axis_index(axis))
    pieces = jax.tree.map(lambda part: lax.all_gather(part, axis), value)
    pieces = jax.tree.map(lambda part: part[::-1], pieces)
    mine = count - 1 - mine
    subtotal = jax.tree.map(
        lambda part, zero: jnp.full_like(part, 0) + jnp.asarray(zero, part.dtype), value, neutral
    )

    def lap(position, subtotal):
        longer = join(subtotal, jax.tree.map(lambda part: part[position], pieces))
        return jax.tree.map(lambda new, old: jnp.where(position < mine, new, old), longer, subtotal)

    return lax.fori_loop(0, count - 1, lap, subtotal)


def entering_2(value, axis, join, neutral):
    place = lax.axis_index(axis)
    gathered = jax.tree.map(
        lambda a, kind: lax.all_gather(a.astype(kind), axis), value, (jnp.bfloat16, jnp.bfloat16)
    )
    state = jax.tree.map(lambda a, e: jnp.zeros_like(a) + jnp.asarray(e, a.dtype), value, neutral)

    def one(lap, state):
        return join(
            state,
            jax.tree.map(
                lambda a, own: lax.dynamic_index_in_dim(a, lap, 0, False).astype(own.dtype),
                gathered,
                value,
            ),
        )

    return lax.fori_loop(0, place, one, state)


def padded_2(value, sides, width):
    for axis, dim in sides:
        size, length = (lax.axis_size(axis), value.shape[dim])
        up = [(i, (i + 1) % size) for i in range(size - 1)]
        down = [(j, i) for i, j in up]
        last = lax.slice_in_dim(value, length - width, length, axis=dim)
        leading = lax.slice_in_dim(value, 0, width, axis=dim)
        before = lax.ppermute(last, axis, up)
        after = lax.ppermute(leading, axis, down)
        value = jnp.concatenate([before, value, after], axis=dim)
    return value


def apply_taps(padded, tap_table, length):
    summed = jnp.zeros((length, padded.shape[1]), jnp.float32)
    for offset in range(tap_table.shape[0]):
        summed = summed + padded[offset : offset + length].astype(jnp.float32) * tap_table[
            offset
        ].astype(jnp.float32)
    return summed


def local_blocks(ssd_x, keys_b, reads_c, timestep_deltas, forgetting_exponent):
    length, groups, per_group, head_dim = ssd_x.shape
    blocks = length // BLOCK
    x_blocks = ssd_x.reshape(blocks, BLOCK, groups, per_group, head_dim)
    b_blocks = keys_b.reshape(blocks, BLOCK, groups, STATE)
    c_blocks = reads_c.reshape(blocks, BLOCK, groups, STATE)
    d_blocks = timestep_deltas.reshape(blocks, BLOCK, groups, per_group)
    l_blocks = forgetting_exponent.reshape(blocks, BLOCK, groups, per_group)
    lower_mask = (jnp.arange(BLOCK)[:, None] >= jnp.arange(BLOCK)[None, :])[None, :, :, None, None]
    running = jnp.cumsum(l_blocks, axis=1)
    log_gaps = jnp.where(lower_mask, running[:, :, None] - running[:, None, :], 0.0)
    decays = jnp.where(lower_mask, jnp.exp(log_gaps), 0.0)
    scores = jnp.einsum("btgn,bsgn->btsg", c_blocks, b_blocks, preferred_element_type=jnp.float32)
    weights = (scores[..., None] * decays * d_blocks[:, None]).astype(jnp.bfloat16)
    within = jnp.einsum("btsgr,bsgrp->btgrp", weights, x_blocks, preferred_element_type=jnp.float32)
    to_end = jnp.exp(running[:, -1:] - running) * d_blocks
    weighted = (x_blocks.astype(jnp.float32) * to_end[..., None]).astype(jnp.bfloat16)
    contribution = jnp.einsum(
        "bsgrp,bsgn->bgrpn", weighted, b_blocks, preferred_element_type=jnp.float32
    )
    return (within, contribution, running, c_blocks)


def combine(earlier, following):
    return (earlier[0] * following[0], earlier[1] * following[0][..., None, None] + following[1])


def run_direction(ssd_x, keys_b, reads_c, timestep_deltas, forgetting_exponent, backward):
    within, contribution, running, c_blocks = local_blocks(
        ssd_x, keys_b, reads_c, timestep_deltas, forgetting_exponent
    )
    block_ends = running[:, -1]

    def chain_step(carry_state, inputs):
        part_state, block_end = inputs
        return (carry_state * jnp.exp(block_end)[..., None, None] + part_state, carry_state)

    summed, before = lax.scan(
        chain_step, jnp.zeros_like(contribution[0]), (contribution, block_ends)
    )
    device_decay = jnp.exp(jnp.sum(block_ends, axis=0))
    identity = (jnp.ones_like(device_decay), jnp.zeros_like(summed))
    if backward:
        incoming = carried_in((device_decay, summed), "sp", combine, identity)
    else:
        incoming = entering_2((device_decay, summed), "sp", combine, identity)
    starts = jnp.cumsum(block_ends, axis=0) - block_ends
    entering = (before + incoming[1][None] * jnp.exp(starts)[..., None, None]).astype(jnp.bfloat16)
    carried = jnp.einsum(
        "btgn,bgrpn->btgrp", c_blocks, entering, preferred_element_type=jnp.float32
    )
    carried = carried * jnp.exp(running)[..., None]
    return (within + carried).reshape(ssd_x.shape)


def local(
    layer_source_rows,
    entry_rescale_factor,
    sliding_mixer_entry_matrix,
    recurrent_mixer_entry_matrix,
    latent_write_read_matrix,
    timestep_matrix,
    sliding_kernel_coefficients,
    recurrent_kernel_coefficients,
    latent_kernel_coefficients,
    lane_forgetting_rate,
    spike_forgetting_rate,
    lane_rescale_factor,
    sliding_mixer_exit_matrix,
    recurrent_mixer_exit_matrix,
):
    float_rows = layer_source_rows.astype(jnp.float32)
    normed = (
        float_rows
        * lax.rsqrt(jnp.mean(float_rows * float_rows, axis=-1, keepdims=True) + epsilon)
        * entry_rescale_factor.astype(jnp.float32)
    ).astype(jnp.bfloat16)
    (
        sliding_mixer_entry_matrix,
        recurrent_mixer_entry_matrix,
        latent_write_read_matrix,
        sliding_mixer_exit_matrix,
        recurrent_mixer_exit_matrix,
    ) = (
        lax.all_gather(sliding_mixer_entry_matrix, "sp", axis=1, tiled=True),
        lax.all_gather(recurrent_mixer_entry_matrix, "sp", axis=1, tiled=True),
        lax.all_gather(latent_write_read_matrix, "sp", axis=1, tiled=True),
        lax.all_gather(sliding_mixer_exit_matrix, "sp", axis=1, tiled=True),
        lax.all_gather(recurrent_mixer_exit_matrix, "sp", axis=1, tiled=True),
    )
    conv_width = sliding_mixer_entry_matrix.shape[2]
    ssd_width = recurrent_mixer_entry_matrix.shape[2]
    state_width = latent_write_read_matrix.shape[2]
    local_heads = timestep_matrix.shape[2]
    step_weight = timestep_matrix.reshape(timestep_matrix.shape[0], 2 * local_heads)
    row_piece = lax.all_gather(normed, "tp", axis=0, tiled=True)
    row_count = row_piece.shape[0]
    conv_cols = jnp.einsum(
        "rd,kdc->rkc", row_piece, sliding_mixer_entry_matrix, preferred_element_type=jnp.float32
    ).reshape(row_count, -1)
    ssd_cols = jnp.einsum(
        "rd,kdc->rkc", row_piece, recurrent_mixer_entry_matrix, preferred_element_type=jnp.float32
    ).reshape(row_count, -1)
    state_cols = jnp.einsum(
        "rd,kdc->rkc", row_piece, latent_write_read_matrix, preferred_element_type=jnp.float32
    ).reshape(row_count, -1)
    step_cols = jnp.dot(row_piece, step_weight, preferred_element_type=jnp.float32)
    projected = jnp.concatenate([conv_cols, ssd_cols, state_cols, step_cols], axis=1).astype(
        jnp.bfloat16
    )
    length = projected.shape[0]
    out_gate = projected[:, :conv_width]
    in_gate = projected[:, conv_width : 2 * conv_width]
    values = projected[:, 2 * conv_width : 3 * conv_width]
    gate_start = 3 * conv_width
    ssd_gate = projected[:, gate_start : gate_start + ssd_width]
    joined = projected[:, gate_start + ssd_width : gate_start + 2 * ssd_width + 2 * state_width]
    raw_step = projected[:, gate_start + 2 * ssd_width + 2 * state_width :].reshape(
        length, 2, local_heads
    )
    gated_in = (in_gate.astype(jnp.float32) * values.astype(jnp.float32)).astype(jnp.bfloat16)
    gated_pad = padded_2(gated_in, (("sp", 0),), 1)
    joined_pad = padded_2(joined, (("sp", 0),), 2)
    y_conv = (
        out_gate.astype(jnp.float32) * apply_taps(gated_pad, sliding_kernel_coefficients, length)
    ).astype(jnp.bfloat16)
    joined_taps = jnp.concatenate(
        [
            recurrent_kernel_coefficients,
            latent_kernel_coefficients.reshape(latent_kernel_coefficients.shape[0], -1),
        ],
        axis=1,
    )
    mixed_ssd = jax.nn.silu(apply_taps(joined_pad, joined_taps, length)).astype(jnp.bfloat16)
    local_groups = state_width // STATE
    per_group = local_heads // local_groups
    ssd_x = mixed_ssd[:, :ssd_width].reshape(length, local_groups, per_group, HEAD_DIM)
    keys_b = mixed_ssd[:, ssd_width : ssd_width + state_width].reshape(length, local_groups, STATE)
    reads_c = mixed_ssd[:, ssd_width + state_width :].reshape(length, local_groups, STATE)
    timestep_deltas = jax.nn.softplus(raw_step.astype(jnp.float32))
    forgetting_exponent = (
        -timestep_deltas * lane_forgetting_rate[None] + spike_forgetting_rate[:, None, :]
    )
    head_shape = (length, local_groups, per_group)
    y_fwd = run_direction(
        ssd_x,
        keys_b,
        reads_c,
        timestep_deltas[:, 0].reshape(head_shape),
        forgetting_exponent[:, 0].reshape(head_shape),
        False,
    )
    y_bwd = jnp.flip(
        run_direction(
            jnp.flip(ssd_x, 0),
            jnp.flip(keys_b, 0),
            jnp.flip(reads_c, 0),
            jnp.flip(timestep_deltas[:, 1].reshape(head_shape), 0),
            jnp.flip(forgetting_exponent[:, 1].reshape(head_shape), 0),
            True,
        ),
        0,
    )
    gated_out = (y_fwd + y_bwd).reshape(length, ssd_width) * jax.nn.silu(
        ssd_gate.astype(jnp.float32)
    )
    grouped = gated_out.reshape(length, local_groups, per_group * HEAD_DIM)
    grouped = grouped * lax.rsqrt(jnp.mean(grouped * grouped, axis=-1, keepdims=True) + epsilon)
    y_ssd = (grouped.reshape(length, ssd_width) * lane_rescale_factor.astype(jnp.float32)).astype(
        jnp.bfloat16
    )
    return lax.psum_scatter(
        (
            jnp.dot(y_conv, sliding_mixer_exit_matrix, preferred_element_type=jnp.float32)
            + jnp.dot(y_ssd, recurrent_mixer_exit_matrix, preferred_element_type=jnp.float32)
        ).astype(jnp.bfloat16),
        "tp",
        scatter_dimension=0,
        tiled=True,
    )


def solution(mesh):
    placed = (
        P(("sp", "tp"), None),
        P(),
        P(None, "sp", "tp"),
        P(None, "sp", "tp"),
        P(None, "sp", "tp"),
        P(None, None, "tp"),
        P(None, "tp"),
        P(None, "tp"),
        P(None, None, "tp"),
        P(None, "tp"),
        P("sp", "tp"),
        P("tp"),
        P("tp", "sp"),
        P("tp", "sp"),
    )
    return jax.shard_map(
        local, mesh=mesh, in_specs=placed, out_specs=P(("sp", "tp"), None), check_vma=False
    )
```

profile of v0, /device:TPU:0, one launch (start us, length us, event | category | flops | bytes accessed | tf_op | source)
XLA Modules:
  0.0 444.4 jit_solution(14916279932055997721)
XLA Ops:
  8.7 2.3 fusion.12
  14.5 26.6 %all-gather.13.cloned.1.call-done = bf16[384,2048]{1,0:T(8,128)(2,1)} async-done(((bf16[192,2048]{1,0:T(8,128)(2,1)}), bf16[384,2048]{1,0:T(8,128)(2,1)}) %all-gather.13.cloned.1.call-update) | async-done | bytes 1572880 | tf_op jit(solution)/shard_map/all_gather | solution.py:167
  43.6 71.1 %fusion.94 = f32[3,128,8,1]{3,2,1,0:T(8,128)S(1)} fusion(f32[3,128,8,1]{3,2,1,0:T(8,128)S(1)} %copy.85), kind=kOutput, calls=%fused_computation.163 | output fusion | flops 390144 | bytes 24576 | tf_op jit(solution)/shard_map/jit(cumsum)/reduce_window_sum | solution.py:81
  115.5 4.6 %fusion.25 = bf16[384,2,512]{2,0,1:T(8,128)(2,1)S(1)} fusion(bf16[2,2048,512]{2,1,0:T(8,128)(2,1)} %all-gather.19.cloned.1.call-done, bf16[384,2048]{1,0:T(8,128)(2,1)} %all-gather.13.cloned.1.call-done), kind=kOutput, calls=%fused_computation.50 | convolution fusion | flops 1611005952 | bytes 6553600 | tf_op jit(solution)/shard_map/rd,kdc->rkc/dot_general | solution.py:172
  120.5 48.3 %all-gather.21.cloned.1.call-done = bf16[2,2048,1024]{2,1,0:T(8,128)(2,1)} async-done(((bf16[2,128,1024]{2,1,0:T(8,128)(2,1)}), bf16[2,2048,1024]{2,1,0:T(8,128)(2,1)}) %all-gather.21.cloned.1.call-update) | async-done | bytes 8388624 | tf_op jit(solution)/shard_map/all_gather | solution.py:158
  168.7 7.9 %convolution_convert_fusion = bf16[384,2,1024]{2,0,1:T(8,128)(2,1)} fusion(bf16[2,2048,1024]{2,1,0:T(8,128)(2,1)} %all-gather.21.cloned.1.call-done, bf16[384,2048]{1,0:T(8,128)(2,1)S(1)} %copy-done.14), kind=kOutput, calls=%fused_computation.34 | convolution fusion | flops 3222011904 | bytes 11534336 | tf_op jit(solution)/shard_map/rd,kdc->rkc/dot_general | solution.py:175
  187.3 11.5 %multiply_convert_fusion = bf16[384,2560]{0,1:T(8,128)(2,1)S(1)} fusion(bf16[384,2560]{0,1:T(8,128)(2,1)} %fusion.7, bf16[2,2560]{0,1:T(8,128)(2,1)S(1)} %copy.80, bf16[2,2560]{0,1:T(8,128)(2,1)S(1)} %copy.78, f32[2560]{0:T(1024)S(1)} %get-tuple-element.354, f32[2560]{0:T(1024)S(1)} %get-tuple-element.355, f32[2560]{0:T(1024)S(1)} %copy-done.16, ...), kind=kLoop, calls=%fused_computation.19 | loop fusion | flops 30474240 | bytes 4003840 | tf_op jit(solution)/shard_map/convert_element_type | solution.py:205
  215.4 15.4 %all-gather.15.cloned.1.call-done = bf16[3,2048,512]{2,1,0:T(8,128)(2,1)} async-done(((bf16[3,128,512]{2,1,0:T(8,128)(2,1)}), bf16[3,2048,512]{2,1,0:T(8,128)(2,1)}) %all-gather.15.cloned.1.call-update) | async-done | bytes 6291472 | tf_op jit(solution)/shard_map/all_gather | solution.py:156
  230.9 6.4 %fusion.22 = bf16[384,3,512]{2,0,1:T(8,128)(2,1)} fusion(bf16[3,2048,512]{2,1,0:T(8,128)(2,1)} %all-gather.15.cloned.1.call-done, bf16[384,2048]{1,0:T(8,128)(2,1)S(1)} %copy-done.15), kind=kOutput, calls=%fused_computation.49 | convolution fusion | flops 2416508928 | bytes 9043968 | tf_op jit(solution)/shard_map/rd,kdc->rkc/dot_general | solution.py:169
  243.9 32.6 %all-reduce = bf16[128]{0:T(256)(128)(2,1)S(1)} all-reduce(bf16[128]{0:T(256)(128)(2,1)S(1)} %dynamic-update-slice), channel_id=2, replica_groups=mesh['sp'=16,'tp'=2] {'sp'}, use_global_device_ids=true, to_apply=%add | all-reduce | flops 128 | bytes 512
  276.6 30.0 %all-reduce.1 = f32[128]{0:T(128)S(1)} all-reduce(f32[128]{0:T(128)S(1)} %exponential_dynamic-update-slice_fusion), channel_id=4, replica_groups=mesh['sp'=16,'tp'=2] {'sp'}, use_global_device_ids=true, to_apply=%add.1 | all-reduce | flops 128 | bytes 1024
  306.7 3.6 fusion.62
  310.3 3.3 reshape.401
  315.9 2.4 copy.98
  320.5 3.6 fusion.37
  324.1 3.7 fusion.36
  328.0 3.2 fusion.32
  331.2 35.6 %all-gather.27.cloned.1.call-done = f32[128,1,64,128]{3,2,1,0:T(8,128)} async-done(((f32[8,1,64,128]{3,2,1,0:T(8,128)}), f32[128,1,64,128]{3,2,1,0:T(8,128)}) %all-gather.27.cloned.1.call-update) | async-done | bytes 4194320 | tf_op jit(solution)/shard_map/all_gather | solution.py:16
  366.8 4.8 %rev.34 = f32[16,8,1,64,128]{4,3,1,2,0:T(8,128)} reverse(f32[16,8,1,64,128]{4,3,1,2,0:T(8,128)} %bitcast.263), dimensions={0} | reverse | bytes 8388608 | tf_op jit(solution)/shard_map/rev | solution.py:17
  371.6 16.4 %while.55 = (s32[]{:T(128)}, f32[8,1,64,128]{3,2,1,0:T(8,128)S(1)}, s32[]{:T(128)}, f32[16,8,1]{1,2,0:T(1,128)S(1)}, f32[16,8,1,64,128]{4,3,1,2,0:T(8,128)}, /*index=5*/s32[]{:T(128)}, s32[]{:T(128)}) while((s32[]{:T(128)}, f32[8,1,64,128]{3,2,1,0:T(8,128)S(1)}, s32[]{:T(128)}, f32[16,8,1]{1,2,0:T(1,128)S(1)}, ...), condition=%wide.region_13.14_spmd.clone, body=%wide.region_12.13_spmd.clone.sunk | while | flops 262148 | bytes 786633 | solution.py:27
  391.2 3.0 rev.35
  397.2 11.3 %all-gather.23.cloned.1.call-done = bf16[512,2048]{1,0:T(8,128)(2,1)} async-done(((bf16[512,128]{1,0:T(8,128)(2,1)}), bf16[512,2048]{1,0:T(8,128)(2,1)}) %all-gather.23.cloned.1.call-update) | async-done | bytes 2097168 | tf_op jit(solution)/shard_map/all_gather | solution.py:160
  408.6 3.9 add_convert_fusion
  412.5 25.4 %reduce-scatter.2.cloned.1.call-done = bf16[192,2048]{1,0:T(8,128)(2,1)} async-done(((bf16[384,2048]{1,0:T(8,128)(2,1)}), bf16[192,2048]{1,0:T(8,128)(2,1)}) %reduce-scatter.2.cloned.1.call-update) | async-done | bytes 786448 | tf_op jit(solution)/shard_map/reduce_scatter | solution.py:243
  (210 shorter events, 69.7 us)
Async XLA Ops:
  6.5 34.5 %copy-start = (bf16[2048,2,8]{0,2,1:T(8,128)(2,1)S(1)}, bf16[2048,2,8]{0,2,1:T(8,128)(2,1)}, u32[]{:S(2)}) copy-start(bf16[2048,2,8]{0,2,1:T(8,128)(2,1)} %param.27) | copy-start | bytes 196612
  6.5 34.5 %all-gather.13.cloned.1.call-start = ((), (), s32[]{:S(2)}) async-start(), calls=%async_computation.1 | async-start | bytes 2359296 | tf_op jit(solution)/shard_map/all_gather | solution.py:167
  8.6 5.1 %copy-start.21 = (bf16[5,512]{1,0:T(8,128)(2,1)S(1)}, bf16[5,512]{1,0:T(8,128)(2,1)}, u32[]{:S(2)}) copy-start(bf16[5,512]{1,0:T(8,128)(2,1)} %param.29) | copy-start | bytes 15364
  8.6 5.1 %copy-start.18 = (bf16[5,2,1024]{2,1,0:T(2,128)(2,1)S(1)}, bf16[5,2,1024]{2,1,0:T(2,128)(2,1)}, u32[]{:S(2)}) copy-start(bf16[5,2,1024]{2,1,0:T(2,128)(2,1)} %param.30) | copy-start | bytes 61444
  8.7 32.4 %copy-start.19 = (f32[384,8]{0,1:T(8,128)S(1)}, f32[384,8]{0,1:T(8,128)}, u32[]{:S(2)}) copy-start(f32[384,8]{0,1:T(8,128)} %param.32) | copy-start | bytes 36868
  8.7 32.4 %copy-start.23 = (f32[2,8]{1,0:T(2,128)S(1)}, f32[2,8]{1,0:T(2,128)}, u32[]{:S(2)}) copy-start(f32[2,8]{1,0:T(2,128)} %param.31) | copy-start | bytes 196
  11.0 104.5 %all-gather.19.cloned.1.call-start = ((), (), s32[]{:S(2)}) async-start(), calls=%async_computation.4 | async-start | bytes 4456448 | tf_op jit(solution)/shard_map/all_gather | solution.py:157
  11.8 157.0 %all-gather.21.cloned.1.call-start = ((), (), s32[]{:S(2)}) async-start(), calls=%async_computation.5 | async-start | bytes 8912896 | tf_op jit(solution)/shard_map/all_gather | solution.py:158
  12.5 218.4 %all-gather.15.cloned.1.call-start = ((), (), s32[]{:S(2)}) async-start(), calls=%async_computation.2 | async-start | bytes 6684672 | tf_op jit(solution)/shard_map/all_gather | solution.py:156
  13.1 293.6 %all-gather.17.cloned.1.call-start = ((), (), s32[]{:S(2)}) async-start(), calls=%async_computation.3 | async-start | bytes 2228224 | tf_op jit(solution)/shard_map/all_gather | solution.py:159
  13.6 314.1 %all-gather.25.cloned.1.call-start = ((), (), s32[]{:S(2)}) async-start(), calls=%async_computation.8 | async-start | bytes 2228224 | tf_op jit(solution)/shard_map/all_gather | solution.py:33
  115.5 53.3 %copy-start.14 = (bf16[384,2048]{1,0:T(8,128)(2,1)S(1)}, bf16[384,2048]{1,0:T(8,128)(2,1)}, u32[]{:S(2)}) copy-start(bf16[384,2048]{1,0:T(8,128)(2,1)} %all-gather.13.cloned.1.call-done) | copy-start | bytes 4718596
  120.5 64.5 %copy-start.3 = (bf16[384,2,512]{0,2,1:T(8,128)(2,1)}, bf16[384,2,512]{0,2,1:T(8,128)(2,1)S(1)}, u32[]{:S(2)}) copy-start(bf16[384,2,512]{0,2,1:T(8,128)(2,1)S(1)} %copy.75) | copy-start | bytes 2359300
  181.1 5.3 %collective-permute-start.2 = (bf16[2,2560]{1,0:T(2,128)(2,1)S(1)}, bf16[2,2560]{1,0:T(2,128)(2,1)S(1)}, u32[]{:S(2)}, u32[]{:S(2)}) collective-permute-start(bf16[2,2560]{1,0:T(2,128)(2,1)S(1)} %copy.77), channel_id=1, source_target_pairs={{0,2},{2,4},{4,6},{6,8},{8,10},{10,12},{12,14},{14,16},{16,18},{18... | collective-permute-start | bytes 30728 | tf_op jit(solution)/shard_map/ppermute | solution.py:57
  183.5 3.3 collective-permute-start.3
  204.6 162.2 %all-gather.27.cloned.1.call-start = ((), (), s32[]{:S(2)}) async-start(), calls=%async_computation.9 | async-start | bytes 4456448 | tf_op jit(solution)/shard_map/all_gather | solution.py:16
  211.8 19.0 %copy-start.15 = (bf16[384,2048]{1,0:T(8,128)(2,1)S(1)}, bf16[384,2048]{1,0:T(8,128)(2,1)}, u32[]{:S(2)}) copy-start(bf16[384,2048]{1,0:T(8,128)(2,1)} %all-gather.13.cloned.1.call-done) | copy-start | bytes 4718596
  212.3 18.5 %copy-start.10 = (f32[3,8,1,64,128]{4,3,1,2,0:T(8,128)}, f32[3,8,1,64,128]{4,3,1,2,0:T(8,128)S(1)}, u32[]{:S(2)}) copy-start(f32[3,8,1,64,128]{4,3,1,2,0:T(8,128)S(1)} %get-tuple-element.202) | copy-start | bytes 2359300
  213.1 195.5 %all-gather.23.cloned.1.call-start = ((), (), s32[]{:S(2)}) async-start(), calls=%async_computation.6 | async-start | bytes 2228224 | tf_op jit(solution)/shard_map/all_gather | solution.py:160
  213.8 224.1 %reduce-scatter.2.cloned.1.call-start = ((), (), s32[]{:S(2)}) async-start(), calls=%async_computation.7 | async-start | bytes 2359296 | tf_op jit(solution)/shard_map/reduce_scatter | solution.py:243
  239.0 67.7 %copy-start.6 = (bf16[384,3,512]{0,2,1:T(8,128)(2,1)}, bf16[384,3,512]{0,2,1:T(8,128)(2,1)S(1)}, u32[]{:S(2)}) copy-start(bf16[384,3,512]{0,2,1:T(8,128)(2,1)S(1)} %copy.74) | copy-start | bytes 3538948
  240.1 66.6 %collective-permute-start = (bf16[1,512]{0,1:T(8,128)(2,1)S(1)}, bf16[1,512]{0,1:T(8,128)(2,1)S(1)}, u32[]{:S(2)}, u32[]{:S(2)}) collective-permute-start(bf16[1,512]{0,1:T(8,128)(2,1)S(1)} %get-tuple-element.402), channel_id=1, source_target_pairs={{0,2},{2,4},{4,6},{6,8},{8,10},{10,12},{12,14},{14,16},{16,18},{18... | collective-permute-start | bytes 3080 | tf_op jit(solution)/shard_map/ppermute | solution.py:57
  242.3 64.4 %collective-permute-start.1 = (bf16[1,512]{0,1:T(8,128)(2,1)S(1)}, bf16[1,512]{0,1:T(8,128)(2,1)S(1)}, u32[]{:S(2)}, u32[]{:S(2)}) collective-permute-start(bf16[1,512]{0,1:T(8,128)(2,1)S(1)} %get-tuple-element.403), channel_id=1, source_target_pairs={{2,0},{4,2},{6,4},{8,6},{10,8},{12,10},{14,12},{16,14},{18,16},{20... | collective-permute-start | bytes 3080 | tf_op jit(solution)/shard_map/ppermute | solution.py:58
  408.6 29.3 %copy-start.1 = (bf16[2048,2,8]{0,2,1:T(8,128)(2,1)S(1)}, bf16[2048,2,8]{0,2,1:T(8,128)(2,1)}, u32[]{:S(2)}) copy-start(bf16[2048,2,8]{0,2,1:T(8,128)(2,1)} %param.27) | copy-start | bytes 196612
  (14 other events, 28.1 us)
Sparse Core Ops, SparseCore 0:
  11.1 29.8 all-gather.12
  43.2 50.3 all-gather.18
  95.9 72.8 all-gather.20
  170.8 60.0 all-gather.14
  232.8 39.8 all-gather.16
  274.8 40.6 all-gather.24
  317.6 49.1 all-gather.26
  368.9 39.5 all-gather.22
  412.6 25.2 reduce-scatter.1
where the time goes:
time: 446 us; the launch traced here: 444 us
  waiting for transfers between devices  166 us (37%)
  other arithmetic  113 us (25%)
  blocking collectives  62.5 us (14%)
  matrix products  41.8 us (9%)
  local copies, waits for them, and re-layouts  38.1 us (9%)
  between operations  14.6 us (3%)
  starting transfers between devices  7.53 us (2%)
    another operation x2, other arithmetic, local_blocks(): running = jnp.cumsum(l_blocks, axis=1)  72.7 us
    unnamed x2, blocking collectives  62.5 us
    all_gather x1, waiting for transfers between devices, local(): lax.all_gather(latent_write_read_matrix, 'sp', axis=1, tiled=True)  48.3 us
    all_gather x1, waiting for transfers between devices, carried_in(): pieces = jax.tree.map(lambda part: lax.all_gather(part, axis), value)  35.6 us
    all_gather x1, waiting for transfers between devices, local(): row_piece = lax.all_gather(normed, 'tp', axis=0, tiled=True)  26.6 us
    reduce_scatter x1, waiting for transfers between devices, local(): lax.psum_scatter((jnp.dot(y_conv, sliding_mixer_exit_matrix, preferred_el...  25.4 us
    select_n x15, other arithmetic, lap(): jnp.where(position < mine, new, old)  15.8 us
    all_gather x1, waiting for transfers between devices, local(): lax.all_gather(sliding_mixer_entry_matrix, 'sp', axis=1, tiled=True)  15.4 us
  transfers between devices with their start and end apart: 13, of which 6 were waited for; matrix products, arithmetic and copies ran while one was open for 41% of the time, Pallas kernels for 0%

commit v1 on v0

v1 whole, which is shorter than its diff:
```python
import jax
import jax.numpy as jnp
from jax import lax
from jax.sharding import PartitionSpec as P

HEAD_DIM = 64
STATE = 128
BLOCK = 128
HALO = 8


epsilon = 1e-05


def swapped(value, axis, distance):
    size = lax.axis_size(axis)
    return lax.ppermute(value, axis, [(i, i ^ distance) for i in range(size)])


def tp_rows(normed):
    if lax.axis_size("tp") != 2:
        return lax.all_gather(normed, "tp", axis=0, tiled=True)
    mine = lax.axis_index("tp")
    count = normed.shape[0]
    other = swapped(normed, "tp", 1)
    rows = jnp.zeros((2 * count, normed.shape[1]), normed.dtype)
    rows = lax.dynamic_update_slice(rows, normed, (mine * count, 0))
    return lax.dynamic_update_slice(rows, other, ((1 - mine) * count, 0))


def with_halo(rows):
    size = lax.axis_size("sp")
    up = [(i, i + 1) for i in range(size - 1)]
    down = [(i + 1, i) for i in range(size - 1)]
    before = lax.ppermute(rows[-HALO:], "sp", up)
    after = lax.ppermute(rows[:HALO], "sp", down)
    return jnp.concatenate([before, rows, after], axis=0)


def apply_taps(padded, tap_table, length):
    taps = tap_table.shape[0]
    first = HALO - taps // 2
    summed = jnp.zeros((length, padded.shape[1]), jnp.float32)
    for offset in range(taps):
        summed = summed + padded[first + offset : first + offset + length].astype(
            jnp.float32
        ) * tap_table[offset].astype(jnp.float32)
    return summed


def decay_levels(decay):
    place = lax.axis_index("sp")
    levels = []
    ahead = jnp.ones_like(decay)
    distance = 1
    while distance < lax.axis_size("sp"):
        other = swapped(decay, "sp", distance)
        upper = (place & distance) != 0
        joins = jnp.stack([upper, ~upper])
        levels.append((distance, joins[:, None], decay, other, ahead))
        ahead = jnp.where(joins[:, None], ahead * other, ahead)
        decay = decay * other
        distance *= 2
    return levels


def entering_state(total, levels):
    place = lax.axis_index("sp")
    prefix = jnp.zeros_like(total)
    for number, (distance, joins, own, other, ahead) in enumerate(levels):
        wide = lambda a: a[..., None, None]
        joins = joins[None, :, :, None]
        if number + 1 < len(levels):
            got = swapped(total.astype(jnp.bfloat16), "sp", distance).astype(jnp.float32)
            prefix = jnp.where(joins, got * wide(ahead) + prefix, prefix)
            total = jnp.where(joins, got * wide(own) + total, total * wide(other) + got)
        else:
            upper = (place & distance) != 0
            send = jnp.where(upper, total[:, 1], total[:, 0]).astype(jnp.bfloat16)
            got = swapped(send, "sp", distance).astype(jnp.float32)
            prefix = jnp.where(joins, got[:, None] * wide(ahead) + prefix, prefix)
    return prefix


def local(
    layer_source_rows,
    entry_rescale_factor,
    sliding_mixer_entry_matrix,
    recurrent_mixer_entry_matrix,
    latent_write_read_matrix,
    timestep_matrix,
    sliding_kernel_coefficients,
    recurrent_kernel_coefficients,
    latent_kernel_coefficients,
    lane_forgetting_rate,
    spike_forgetting_rate,
    lane_rescale_factor,
    sliding_mixer_exit_matrix,
    recurrent_mixer_exit_matrix,
):
    f32, bf16 = jnp.float32, jnp.bfloat16
    conv_width = sliding_mixer_entry_matrix.shape[2]
    ssd_width = recurrent_mixer_entry_matrix.shape[2]
    state_width = latent_write_read_matrix.shape[2]
    heads = timestep_matrix.shape[2]
    assert state_width == heads * STATE and ssd_width == heads * HEAD_DIM

    ssd_shard = jnp.concatenate(
        [
            recurrent_mixer_entry_matrix[0],
            recurrent_mixer_entry_matrix[1],
            latent_write_read_matrix[0],
            latent_write_read_matrix[1],
        ],
        axis=1,
    )
    ssd_weight = lax.all_gather(ssd_shard, "sp", axis=0, tiled=True)

    float_rows = layer_source_rows.astype(f32)
    normed = (
        float_rows
        * lax.rsqrt(jnp.mean(float_rows * float_rows, axis=-1, keepdims=True) + epsilon)
        * entry_rescale_factor.astype(f32)
    ).astype(bf16)
    rows = tp_rows(normed)
    length = rows.shape[0]

    exit_shard = jnp.concatenate(
        [sliding_mixer_exit_matrix, recurrent_mixer_exit_matrix], axis=0
    ).T
    conv_shard = jnp.concatenate(
        [sliding_mixer_entry_matrix[k] for k in range(3)] + [exit_shard], axis=1
    )
    conv_shard, rows = lax.optimization_barrier((conv_shard, rows))
    conv_weight = lax.all_gather(conv_shard, "sp", axis=0, tiled=True)

    wide_rows = with_halo(rows)

    raw_step = (
        jnp.dot(rows, timestep_matrix.reshape(-1, 2 * heads), preferred_element_type=f32)
        .astype(bf16)
        .astype(f32)
        .reshape(length, 2, heads)
    )
    deltas = jax.nn.softplus(raw_step)
    log_decay = -deltas * lane_forgetting_rate[None] + spike_forgetting_rate[:, None, :]
    blocks = length // BLOCK
    order = jnp.arange(BLOCK)
    lower = (order[:, None] >= order[None, :]).astype(f32)
    sums = jnp.stack([lower, lower.T])
    logs = log_decay.reshape(blocks, BLOCK, 2, heads).transpose(2, 3, 0, 1)
    delta = deltas.reshape(blocks, BLOCK, 2, heads).transpose(2, 3, 0, 1)
    running = jnp.einsum("dhbs,dts->dhbt", logs, sums, precision=lax.Precision.HIGHEST)
    ends = jnp.stack([running[0, :, :, -1], running[1, :, :, 0]])
    to_end = jnp.exp(ends[..., None] - running) * delta
    levels = decay_levels(jnp.exp(jnp.sum(ends, axis=-1)))
    levels = [(n, j, a.T, b.T, c.T) for n, j, a, b, c in levels]
    before_ends = jnp.cumsum(ends[0], axis=-1) - ends[0]
    after_ends = jnp.cumsum(ends[1][:, ::-1], axis=-1)[:, ::-1] - ends[1]
    starts = jnp.exp(jnp.stack([before_ends, after_ends]))
    mask = order[:, None] >= order[None, :]
    gaps = running[..., :, None] - running[..., None, :]
    decays = (
        jnp.where(mask, jnp.exp(jnp.where(mask, gaps[0], 0.0)), 0.0) * delta[0][..., None, :]
        + jnp.where(mask.T, jnp.exp(jnp.where(mask.T, gaps[1], 0.0)), 0.0)
        * delta[1][..., None, :]
    )

    projected = jnp.dot(wide_rows, ssd_weight, preferred_element_type=f32).astype(bf16)
    ssd_gate = projected[HALO : HALO + length, :ssd_width]
    joined_taps = jnp.concatenate(
        [
            recurrent_kernel_coefficients,
            latent_kernel_coefficients.reshape(latent_kernel_coefficients.shape[0], -1),
        ],
        axis=1,
    )
    mixed = jax.nn.silu(apply_taps(projected[:, ssd_width:], joined_taps, length)).astype(bf16)
    ssd_x = mixed[:, :ssd_width].reshape(blocks, BLOCK, heads, HEAD_DIM)
    keys_b = mixed[:, ssd_width : ssd_width + state_width].reshape(blocks, BLOCK, heads, STATE)
    reads_c = mixed[:, ssd_width + state_width :].reshape(blocks, BLOCK, heads, STATE)
    ssd_x = ssd_x.transpose(2, 0, 1, 3)
    keys_b = keys_b.transpose(2, 0, 1, 3)
    reads_c = reads_c.transpose(2, 0, 1, 3)

    x_float = ssd_x.astype(f32)
    weighted = jnp.concatenate(
        [(x_float * to_end[d][..., None]).astype(bf16) for d in range(2)], axis=-1
    )
    contribution = jnp.einsum("hbsp,hbsn->hbpn", weighted, keys_b, preferred_element_type=f32)
    contribution = contribution.reshape(heads, blocks, 2, HEAD_DIM, STATE)
    end_decay = jnp.exp(ends)[..., None, None]
    forward, fore = [], jnp.zeros((heads, HEAD_DIM, STATE), f32)
    for b in range(blocks):
        forward.append(fore)
        fore = fore * end_decay[0, :, b] + contribution[:, b, 0]
    backward, aft = [None] * blocks, jnp.zeros((heads, HEAD_DIM, STATE), f32)
    for b in reversed(range(blocks)):
        backward[b] = aft
        aft = aft * end_decay[1, :, b] + contribution[:, b, 1]
    prefix = entering_state(jnp.stack([fore, aft], axis=1), levels)

    scores = jnp.einsum("hbtn,hbsn->hbts", reads_c, keys_b, preferred_element_type=f32)
    within = jnp.einsum(
        "hbts,hbsp->hbtp", (scores * decays).astype(bf16), ssd_x, preferred_element_type=f32
    )
    inside = jnp.stack([jnp.stack(forward, 1), jnp.stack(backward, 1)], axis=2)
    entering = inside + prefix[:, None] * starts.transpose(1, 2, 0)[..., None, None]
    entering = entering.astype(bf16).reshape(heads, blocks, 2 * HEAD_DIM, STATE)
    carried = jnp.einsum("hbtn,hbpn->hbtp", reads_c, entering, preferred_element_type=f32)
    grown = jnp.exp(running)[..., None]
    y = within + carried[..., :HEAD_DIM] * grown[0] + carried[..., HEAD_DIM:] * grown[1]
    gate = ssd_gate.astype(f32).reshape(blocks, BLOCK, heads, HEAD_DIM).transpose(2, 0, 1, 3)
    y = y * jax.nn.silu(gate)
    y = y * lax.rsqrt(jnp.mean(y * y, axis=-1, keepdims=True) + epsilon)
    y = y * lane_rescale_factor.astype(f32).reshape(heads, 1, 1, HEAD_DIM)
    y_ssd = y.astype(bf16).transpose(1, 2, 0, 3).reshape(length, ssd_width)

    conv = jnp.dot(
        wide_rows, conv_weight[:, : 3 * conv_width], preferred_element_type=f32
    ).astype(bf16)
    out_gate = conv[HALO : HALO + length, :conv_width].astype(f32)
    gated_in = (
        conv[:, conv_width : 2 * conv_width].astype(f32) * conv[:, 2 * conv_width :].astype(f32)
    ).astype(bf16)
    y_conv = (out_gate * apply_taps(gated_in, sliding_kernel_coefficients, length)).astype(bf16)

    mixed_y = jnp.concatenate([y_conv, y_ssd], axis=1)
    exit_weight = conv_weight[:, 3 * conv_width :]

    def leave(part):
        return lax.dot_general(
            part, exit_weight, (((1,), (1,)), ((), ())), preferred_element_type=f32
        ).astype(bf16)

    if lax.axis_size("tp") != 2:
        return lax.psum_scatter(leave(mixed_y), "tp", scatter_dimension=0, tiled=True)
    mine = lax.axis_index("tp")
    half = length // 2
    sent = leave(lax.dynamic_slice_in_dim(mixed_y, (1 - mine) * half, half, 0))
    got = swapped(sent, "tp", 1)
    kept = leave(lax.dynamic_slice_in_dim(mixed_y, mine * half, half, 0))
    return (kept.astype(f32) + got.astype(f32)).astype(bf16)


def solution(mesh):
    placed = (
        P(("sp", "tp"), None),
        P(),
        P(None, "sp", "tp"),
        P(None, "sp", "tp"),
        P(None, "sp", "tp"),
        P(None, None, "tp"),
        P(None, "tp"),
        P(None, "tp"),
        P(None, None, "tp"),
        P(None, "tp"),
        P("sp", "tp"),
        P("tp"),
        P("tp", "sp"),
        P("tp", "sp"),
    )
    return jax.shard_map(
        local, mesh=mesh, in_specs=placed, out_specs=P(("sp", "tp"), None), check_vma=False
    )
```

time: 446 us -> 283 us (0.63)
  other arithmetic: 113 us -> 25.2 us
  blocking collectives: 62.5 us -> 0 us
  matrix products: 41.8 us -> 30.1 us
  starting transfers between devices: 7.53 us -> 18.4 us
  local copies, waits for them, and re-layouts: 38.1 us -> 29 us
    another operation x4 -> x10, other arithmetic: 72.8 us -> 2.73 us  [the longest x2 1.31 us: local(): inside = jnp.stack([jnp.stack(forward, 1), jnp.stack(backward, 1)], axis=2)]
    unnamed x2 -> x0, blocking collectives: 62.5 us -> none
    ppermute x4 -> x11, waiting for transfers between devices: 0.01 us -> 44 us  [the longest x9 44 us: swapped(): return lax.ppermute(value, axis, [(i, i ^ distance) for i in range(size)])]
    reduce_scatter x1 -> x0, waiting for transfers between devices: 25.4 us -> none  [local(): lax.psum_scatter((jnp.dot(y_conv, sliding_mixer_exit_matrix, preferred_el...]
    all_gather x8 -> x2, waiting for transfers between devices: 137 us -> 122 us  [the longest x1 68.2 us: local(): conv_weight = lax.all_gather(conv_shard, 'sp', axis=0, tiled=True)]
    select_n x15 -> x2, other arithmetic: 15.8 us -> 2.74 us  [the longest x1 1.44 us: entering_state(): total = jnp.where(joins, got * wide(own) + total, total * wide(other) + got)]
    another operation x16 -> x7, local copies, waits for them, and re-layouts: 13.1 us -> 0.06 us  [the longest x5 0.03 us: local(): ends = jnp.stack([running[0, :, :, -1], running[1, :, :, 0]])]
    dot_general x12 -> x9, matrix products: 41.8 us -> 30.1 us  [the longest x1 8.68 us: local(): jnp.dot(wide_rows, ssd_weight, preferred_element_type=f32).astype(bf16)]
  transfers between devices with their start and end apart: 13 -> 13, of which waited for: 6 -> 9; matrix products, arithmetic and copies ran while one was open for 41% -> 21% of each run, Pallas kernels for 0% -> 0%
where the time goes in v1:
time: 283 us
  waiting for transfers between devices  166 us (59%)
  matrix products  30.1 us (11%)
  local copies, waits for them, and re-layouts  29 us (10%)
  other arithmetic  25.2 us (9%)
  starting transfers between devices  18.4 us (7%)
  between operations  14.2 us (5%)
    all_gather x1, waiting for transfers between devices, local(): conv_weight = lax.all_gather(conv_shard, 'sp', axis=0, tiled=True)  68.2 us
    all_gather x1, waiting for transfers between devices, local(): ssd_weight = lax.all_gather(ssd_shard, 'sp', axis=0, tiled=True)  53.7 us
    ppermute x9, waiting for transfers between devices, swapped(): return lax.ppermute(value, axis, [(i, i ^ distance) for i in range(size)])  44 us
    ppermute x9, starting transfers between devices, swapped(): return lax.ppermute(value, axis, [(i, i ^ distance) for i in range(size)])  14.7 us
    unnamed x88, local copies, waits for them, and re-layouts  9.58 us
    dot_general x1, matrix products, local(): jnp.dot(wide_rows, ssd_weight, preferred_element_type=f32).astype(bf16)  8.68 us
    dot_general x2, matrix products, leave(): lax.dot_general(part, exit_weight, (((1,), (1,)), ((), ())), preferred_el...  7.31 us
    dot_general x1, matrix products, local(): jnp.dot(wide_rows, conv_weight[:, :3 * conv_width], preferred_element_typ...  6.02 us
  transfers between devices with their start and end apart: 13, of which 9 were waited for; matrix products, arithmetic and copies ran while one was open for 21% of the time, Pallas kernels for 0%

profile of v1, /device:TPU:0, one launch (start us, length us, event | category | flops | bytes accessed | tf_op | source)
XLA Modules:
  0.0 282.8 jit_solution(1260736302038786378)
XLA Ops:
  10.5 3.0 %collective-permute-start = (bf16[192,2048]{1,0:T(8,128)(2,1)S(1)}, bf16[192,2048]{1,0:T(8,128)(2,1)S(1)}, u32[]{:S(2)}, u32[]{:S(2)}) collective-permute-start(bf16[192,2048]{1,0:T(8,128)(2,1)S(1)} %get-tuple-element.25), channel_id=1, source_target_pairs={{0,1},{1,0},{2,3},{3,2},{4,5},{5,4},{6,7},{7,6},{8,9},{9,8},{10,11... | collective-permute-start | bytes 2359304 | tf_op jit(solution)/shard_map/ppermute | solution.py:17
  13.5 1.8 fusion.125
  19.1 1.8 pad_maximum_fusion.2
  21.0 10.1 %collective-permute-done = bf16[192,2048]{1,0:T(8,128)(2,1)S(1)} collective-permute-done((bf16[192,2048]{1,0:T(8,128)(2,1)S(1)}, bf16[192,2048]{1,0:T(8,128)(2,1)S(1)}, u32[]{:S(2)}, u32[]{:S(2)}) %collective-permute-start) | collective-permute-done | bytes 786464 | tf_op jit(solution)/shard_map/ppermute | solution.py:17
  35.4 2.4 collective-permute-start.1
  42.0 2.2 broadcast_subtract_fusion
  44.7 3.6 %collective-permute-start.6 = (f32[2,8]{1,0:T(2,128)S(1)}, f32[2,8]{1,0:T(2,128)S(1)}, u32[]{:S(2)}, u32[]{:S(2)}) collective-permute-start(f32[2,8]{1,0:T(2,128)S(1)} %get-tuple-element.64), channel_id=1, source_target_pairs={{0,4},{2,6},{4,0},{6,2},{8,12},{10,14},{12,8},{14,10},{16,20},{18,... | collective-permute-start | bytes 200 | tf_op jit(solution)/shard_map/ppermute | solution.py:17
  49.9 3.0 %collective-permute-start.8 = (f32[2,8]{1,0:T(2,128)S(1)}, f32[2,8]{1,0:T(2,128)S(1)}, u32[]{:S(2)}, u32[]{:S(2)}) collective-permute-start(f32[2,8]{1,0:T(2,128)S(1)} %mul.523), channel_id=1, source_target_pairs={{0,8},{2,10},{4,12},{6,14},{8,0},{10,2},{12,4},{14,6},{16,24},{18,... | collective-permute-start | bytes 200 | tf_op jit(solution)/shard_map/ppermute | solution.py:17
  59.7 53.7 %all-gather.5.cloned.1.call-done = bf16[2048,3072]{1,0:T(8,128)(2,1)} async-done(((bf16[128,3072]{1,0:T(8,128)(2,1)}), bf16[2048,3072]{1,0:T(8,128)(2,1)}) %all-gather.5.cloned.1.call-update) | async-done | bytes 12582928 | tf_op jit(solution)/shard_map/all_gather | solution.py:117
  113.4 8.7 %convolution_convert_fusion = bf16[400,3072]{1,0:T(8,128)(2,1)S(1)} fusion(bf16[400,2048]{1,0:T(8,128)(2,1)} %constant_dynamic-update-slice_fusion, bf16[2048,3072]{1,0:T(8,128)(2,1)} %all-gather.5.cloned.1.call-done), kind=kOutput, calls=%fused_computation.2 | convolution fusion | flops 5034393600 | bytes 16678912 | tf_op jit(solution)/shard_map/dot_general | solution.py:169
  122.1 4.2 %multiply_convert_fusion = bf16[384,2560]{1,0:T(8,128)(2,1)} fusion(bf16[400,3072]{1,0:T(8,128)(2,1)S(1)} %convolution_convert_fusion, f32[2560]{0:T(1024)S(1)} %get-tuple-element.10, f32[2560]{0:T(1024)S(1)} %get-tuple-element.11, f32[2560]{0:T(1024)S(1)} %get-tuple-element.12, f32[2560]{0:T(1024)S(1)} %get-tuple-element.13, f32[2560]{0:T(1024)S(1)} %get-tuple-element.9), kind=kLoop, calls=%fused_computation.3 | loop fusion | flops 18677760 | bytes 11847680 | tf_op jit(solution)/shard_map/convert_element_type | solution.py:178
  126.3 1.8 slice.271
  128.0 1.7 reshape.312
  131.0 2.4 slice_bitcast_fusion.3
  136.0 68.2 %all-gather.3.cloned.1.call-done = bf16[2048,2560]{0,1:T(8,128)(2,1)} async-done(((bf16[128,2560]{0,1:T(8,128)(2,1)}), bf16[2048,2560]{0,1:T(8,128)(2,1)}) %all-gather.3.cloned.1.call-update) | async-done | bytes 10485776 | tf_op jit(solution)/shard_map/all_gather | solution.py:135
  204.2 6.0 %fusion.6 = bf16[400,1536]{1,0:T(8,128)(2,1)S(1)} fusion(bf16[400,2048]{1,0:T(8,128)(2,1)} %constant_dynamic-update-slice_fusion, bf16[2048,2560]{0,1:T(8,128)(2,1)} %all-gather.3.cloned.1.call-done), kind=kOutput, calls=%fused_computation.8 | convolution fusion | flops 2517196800 | bytes 9158656 | tf_op jit(solution)/shard_map/dot_general | solution.py:219
  213.3 5.8 %collective-permute-done.5 = bf16[8,2,64,128]{3,2,1,0:T(8,128)(2,1)S(1)} collective-permute-done((bf16[8,2,64,128]{3,2,1,0:T(8,128)(2,1)S(1)}, bf16[8,2,64,128]{3,2,1,0:T(8,128)(2,1)S(1)}, u32[]{:S(2)}, u32[]{:S(2)}) %collective-permute-start.5) | collective-permute-done | bytes 262176 | tf_op jit(solution)/shard_map/ppermute | solution.py:17
  225.4 2.8 collective-permute-done.7
  231.4 6.0 %collective-permute-done.9 = bf16[8,64,128]{2,1,0:T(8,128)(2,1)S(1)} collective-permute-done((bf16[8,64,128]{2,1,0:T(8,128)(2,1)S(1)}, bf16[8,64,128]{2,1,0:T(8,128)(2,1)S(1)}, u32[]{:S(2)}, u32[]{:S(2)}) %collective-permute-start.9) | collective-permute-done | bytes 131104 | tf_op jit(solution)/shard_map/ppermute | solution.py:17
  239.8 1.8 fusion.49
  241.7 5.2 %multiply_reduce_fusion = (f32[8,3,128]{2,1,0:T(4,128)}, f32[8,3,128,64]{2,3,1,0:T(8,128)}) fusion(f32[3,128,8,64]{1,3,0,2:T(8,128)} %copy.135, f32[8,3,128]{2,1,0:T(4,128)} %copy.133, f32[8,3,128,128]{2,3,1,0:T(8,128)} %fusion.49, f32[8,3,128]{2,1,0:T(4,128)} %copy.132, bf16[3,128,8,64]{1,3,0,2:T(8,128)(2,1)S(1)} %copy-done.9, ...), kind=kOutput, calls=%fused_computation.73 | convolution fusion | flops 156693504 | bytes 8351744 | tf_op jit(solution)/shard_map/hbts,hbsp->hbtp/dot_general | solution.py:204
  249.9 3.2 %fusion.15 = bf16[192,2048]{1,0:T(8,128)(2,1)S(1)} fusion(bf16[2048,2560]{0,1:T(8,128)(2,1)} %all-gather.3.cloned.1.call-done, s32[]{:T(128)S(6)} %select_n.69, bf16[384,512]{1,0:T(8,128)(2,1)S(1)} %copy-done.13, bf16[384,512]{1,0:T(8,128)(2,1)S(1)} %reshape.314), kind=kOutput, calls=%fused_computation.11 | convolution fusion | flops 806486016 | bytes 5767172 | tf_op jit(solution)/shard_map/dot_general | solution.py:232
  254.6 17.2 %collective-permute-done.10 = bf16[192,2048]{1,0:T(8,128)(2,1)S(1)} collective-permute-done((bf16[192,2048]{1,0:T(8,128)(2,1)S(1)}, bf16[192,2048]{1,0:T(8,128)(2,1)S(1)}, u32[]{:S(2)}, u32[]{:S(2)}) %collective-permute-start.10) | collective-permute-done | bytes 786464 | tf_op jit(solution)/shard_map/ppermute | solution.py:17
  271.8 4.1 %add_convert_fusion = bf16[192,2048]{1,0:T(8,128)(2,1)} fusion(bf16[192,2048]{1,0:T(8,128)(2,1)S(1)} %collective-permute-done.10, bf16[2048,2560]{0,1:T(8,128)(2,1)} %all-gather.3.cloned.1.call-done, s32[]{:T(128)S(6)} %select_n.68, bf16[384,512]{1,0:T(8,128)(2,1)S(1)} %copy-done.13, bf16[384,512]{1,0:T(8,128)(2,1)S(1)} %reshape.314), kind=kOutput, calls=%fused_computation.33 | convolution fusion | flops 808058880 | bytes 6553604 | tf_op jit(solution)/shard_map/dot_general | solution.py:232
  (196 shorter events, 48.0 us)
Async XLA Ops:
  6.5 27.6 %copy-start = (bf16[2048,2,8]{0,2,1:T(8,128)(2,1)S(1)}, bf16[2048,2,8]{0,2,1:T(8,128)(2,1)}, u32[]{:S(2)}) copy-start(bf16[2048,2,8]{0,2,1:T(8,128)(2,1)} %param.19) | copy-start | bytes 196612
  6.5 106.9 %all-gather.5.cloned.1.call-start = ((), (), s32[]{:S(2)}) async-start(), calls=%async_computation.1 | async-start | bytes 13369344 | tf_op jit(solution)/shard_map/all_gather | solution.py:117
  9.7 194.5 %all-gather.3.cloned.1.call-start = ((), (), s32[]{:S(2)}) async-start(), calls=%async_computation | async-start | bytes 11141120 | tf_op jit(solution)/shard_map/all_gather | solution.py:135
  10.5 20.6 %collective-permute-start = (bf16[192,2048]{1,0:T(8,128)(2,1)S(1)}, bf16[192,2048]{1,0:T(8,128)(2,1)S(1)}, u32[]{:S(2)}, u32[]{:S(2)}) collective-permute-start(bf16[192,2048]{1,0:T(8,128)(2,1)S(1)} %get-tuple-element.25), channel_id=1, source_target_pairs={{0,1},{1,0},{2,3},{3,2},{4,5},{5,4},{6,7},{7,6},{8,9},{9,8},{10,11... | collective-permute-start | bytes 2359304 | tf_op jit(solution)/shard_map/ppermute | solution.py:17
  19.1 12.1 %copy-start.14 = (bf16[5,2,1024]{2,1,0:T(2,128)(2,1)S(1)}, bf16[5,2,1024]{2,1,0:T(2,128)(2,1)}, u32[]{:S(2)}) copy-start(bf16[5,2,1024]{2,1,0:T(2,128)(2,1)} %param.22) | copy-start | bytes 61444
  19.1 12.1 %copy-start.35 = (bf16[512]{0:T(512)(128)(2,1)S(1)}, bf16[512]{0:T(512)(128)(2,1)}, u32[]{:S(2)}) copy-start(bf16[512]{0:T(512)(128)(2,1)} %param.25) | copy-start | bytes 3076
  19.1 13.6 %copy-start.29 = (bf16[5,512]{1,0:T(8,128)(2,1)S(1)}, bf16[5,512]{1,0:T(8,128)(2,1)}, u32[]{:S(2)}) copy-start(bf16[5,512]{1,0:T(8,128)(2,1)} %param.21) | copy-start | bytes 15364
  19.1 14.4 %copy-start.23 = (bf16[3,512]{1,0:T(4,128)(2,1)S(1)}, bf16[3,512]{1,0:T(4,128)(2,1)}, u32[]{:S(2)}) copy-start(bf16[3,512]{1,0:T(4,128)(2,1)} %param.20) | copy-start | bytes 9220
  32.0 22.5 %copy-start.21 = (pred[2]{0:T(512)(128)(4,1)}, pred[2]{0:T(512)(128)(4,1)S(1)}, u32[]{:S(2)}) copy-start(pred[2]{0:T(512)(128)(4,1)S(1)} %pad_add_fusion.3) | copy-start | bytes 10
  32.1 22.4 %copy-start.24 = (pred[2]{0:T(512)(128)(4,1)}, pred[2]{0:T(512)(128)(4,1)S(1)}, u32[]{:S(2)}) copy-start(pred[2]{0:T(512)(128)(4,1)S(1)} %pad_add_fusion.2) | copy-start | bytes 10
  32.1 22.3 %copy-start.30 = (pred[2]{0:T(512)(128)(4,1)}, pred[2]{0:T(512)(128)(4,1)S(1)}, u32[]{:S(2)}) copy-start(pred[2]{0:T(512)(128)(4,1)S(1)} %pad_add_fusion.1) | copy-start | bytes 10
  35.2 9.5 %collective-permute-start.4 = (f32[2,8]{1,0:T(2,128)S(1)}, f32[2,8]{1,0:T(2,128)S(1)}, u32[]{:S(2)}, u32[]{:S(2)}) collective-permute-start(f32[2,8]{1,0:T(2,128)S(1)} %exp.52), channel_id=1, source_target_pairs={{0,2},{2,0},{4,6},{6,4},{8,10},{10,8},{12,14},{14,12},{16,18},{18,... | collective-permute-start | bytes 200 | tf_op jit(solution)/shard_map/ppermute | solution.py:17
  35.4 21.8 %collective-permute-start.1 = (bf16[8,2048]{1,0:T(8,128)(2,1)S(1)}, bf16[8,2048]{1,0:T(8,128)(2,1)S(1)}, u32[]{:S(2)}, u32[]{:S(2)}) collective-permute-start(bf16[8,2048]{1,0:T(8,128)(2,1)S(1)} %get-tuple-element.32), channel_id=1, source_target_pairs={{0,2},{2,4},{4,6},{6,8},{8,10},{10,12},{12,14},{14,16},{16,18},{18... | collective-permute-start | bytes 98312 | tf_op jit(solution)/shard_map/ppermute | solution.py:35
  37.8 21.3 %collective-permute-start.2 = (bf16[8,2048]{1,0:T(8,128)(2,1)S(1)}, bf16[8,2048]{1,0:T(8,128)(2,1)S(1)}, u32[]{:S(2)}, u32[]{:S(2)}) collective-permute-start(bf16[8,2048]{1,0:T(8,128)(2,1)S(1)} %get-tuple-element.31), channel_id=1, source_target_pairs={{2,0},{4,2},{6,4},{8,6},{10,8},{12,10},{14,12},{16,14},{18,16},{20... | collective-permute-start | bytes 98312 | tf_op jit(solution)/shard_map/ppermute | solution.py:36
  44.7 5.2 %collective-permute-start.6 = (f32[2,8]{1,0:T(2,128)S(1)}, f32[2,8]{1,0:T(2,128)S(1)}, u32[]{:S(2)}, u32[]{:S(2)}) collective-permute-start(f32[2,8]{1,0:T(2,128)S(1)} %get-tuple-element.64), channel_id=1, source_target_pairs={{0,4},{2,6},{4,0},{6,2},{8,12},{10,14},{12,8},{14,10},{16,20},{18,... | collective-permute-start | bytes 200 | tf_op jit(solution)/shard_map/ppermute | solution.py:17
  49.9 4.5 %collective-permute-start.8 = (f32[2,8]{1,0:T(2,128)S(1)}, f32[2,8]{1,0:T(2,128)S(1)}, u32[]{:S(2)}, u32[]{:S(2)}) collective-permute-start(f32[2,8]{1,0:T(2,128)S(1)} %mul.523), channel_id=1, source_target_pairs={{0,8},{2,10},{4,12},{6,14},{8,0},{10,2},{12,4},{14,6},{16,24},{18,... | collective-permute-start | bytes 200 | tf_op jit(solution)/shard_map/ppermute | solution.py:17
  135.7 74.6 %copy-start.22 = (pred[2]{0:T(512)(128)(4,1)S(1)}, pred[2]{0:T(512)(128)(4,1)}, u32[]{:S(2)}) copy-start(pred[2]{0:T(512)(128)(4,1)} %copy-done.21) | copy-start | bytes 10
  135.7 74.5 %collective-permute-start.3 = (bf16[8,2,64,128]{3,2,1,0:T(8,128)(2,1)S(1)}, bf16[8,2,64,128]{3,2,1,0:T(8,128)(2,1)S(1)}, u32[]{:S(2)}, u32[]{:S(2)}) collective-permute-start(bf16[8,2,64,128]{3,2,1,0:T(8,128)(2,1)S(1)} %fusion.70), channel_id=1, source_target_pairs={{0,2},{2,0},{4,6},{6,4},{8,10},{10,8},{12,14},{14,12},{16,18},{18,... | collective-permute-start | bytes 786440 | tf_op jit(solution)/shard_map/ppermute | solution.py:17
  210.6 8.5 %copy-start.25 = (pred[2]{0:T(512)(128)(4,1)S(1)}, pred[2]{0:T(512)(128)(4,1)}, u32[]{:S(2)}) copy-start(pred[2]{0:T(512)(128)(4,1)} %copy-done.24) | copy-start | bytes 10
  210.6 8.5 %collective-permute-start.5 = (bf16[8,2,64,128]{3,2,1,0:T(8,128)(2,1)S(1)}, bf16[8,2,64,128]{3,2,1,0:T(8,128)(2,1)S(1)}, u32[]{:S(2)}, u32[]{:S(2)}) collective-permute-start(bf16[8,2,64,128]{3,2,1,0:T(8,128)(2,1)S(1)} %fusion.118), channel_id=1, source_target_pairs={{0,4},{2,6},{4,0},{6,2},{8,12},{10,14},{12,8},{14,10},{16,20},{18,... | collective-permute-start | bytes 786440 | tf_op jit(solution)/shard_map/ppermute | solution.py:17
  213.3 7.9 %copy-start.6 = (bf16[48,8,8,128]{3,1,2,0:T(8,128)(2,1)S(1)}, bf16[48,8,8,128]{3,1,2,0:T(8,128)(2,1)}, u32[]{:S(2)}) copy-start(bf16[48,8,8,128]{3,1,2,0:T(8,128)(2,1)} %get-tuple-element.26) | copy-start | bytes 2359300
  220.2 7.9 %collective-permute-start.7 = (bf16[8,2,64,128]{3,2,1,0:T(8,128)(2,1)}, bf16[8,2,64,128]{3,2,1,0:T(8,128)(2,1)}, u32[]{:S(2)}, u32[]{:S(2)}) collective-permute-start(bf16[8,2,64,128]{3,2,1,0:T(8,128)(2,1)} %fusion.90), channel_id=1, source_target_pairs={{0,8},{2,10},{4,12},{6,14},{8,0},{10,2},{12,4},{14,6},{16,24},{18,... | collective-permute-start | bytes 786440 | tf_op jit(solution)/shard_map/ppermute | solution.py:17
  229.6 7.7 %collective-permute-start.9 = (bf16[8,64,128]{2,1,0:T(8,128)(2,1)S(1)}, bf16[8,64,128]{2,1,0:T(8,128)(2,1)S(1)}, u32[]{:S(2)}, u32[]{:S(2)}) collective-permute-start(bf16[8,64,128]{2,1,0:T(8,128)(2,1)S(1)} %fusion.88), channel_id=1, source_target_pairs={{0,16},{2,18},{4,20},{6,22},{8,24},{10,26},{12,28},{14,30},{16,0},... | collective-permute-start | bytes 393224 | tf_op jit(solution)/shard_map/ppermute | solution.py:17
  253.1 18.8 %collective-permute-start.10 = (bf16[192,2048]{1,0:T(8,128)(2,1)S(1)}, bf16[192,2048]{1,0:T(8,128)(2,1)S(1)}, u32[]{:S(2)}, u32[]{:S(2)}) collective-permute-start(bf16[192,2048]{1,0:T(8,128)(2,1)S(1)} %fusion.15), channel_id=1, source_target_pairs={{0,1},{1,0},{2,3},{3,2},{4,5},{5,4},{6,7},{7,6},{8,9},{9,8},{10,11... | collective-permute-start | bytes 2359304 | tf_op jit(solution)/shard_map/ppermute | solution.py:17
  (28 other events, 83.3 us)
Sparse Core Ops, SparseCore 0:
  9.8 103.5 all-gather.4
  115.5 88.5 all-gather.2
